TPU v7x, 512 devices: a whole 4x4x16 slice. The times are simulated.
512 devices in a mesh: gr: 2 (over z_hi), fs: 32 (over z_lo, y), tp: 8 (over x, core).
Axes of the slice: x: 4, y: 4, z: 16 (z_hi: 2, z_lo: 8; z = z_hi * 8 + z_lo), core: 2. Of those that a mesh axis runs over, the one named last changes fastest.
Arguments:
- prompt: bfloat16 [8192, 2048], P(('gr', 'tp'), 'fs'), may hold values from -2.5 to 2.5
- gain_pre: float32 [2048], P(('gr', 'fs')), may hold values from 0.1 to 1.9
- gate_pre: float32 [2048, 5632], P(('gr', 'fs'), 'tp'), may hold values from -6 to 6
- up_pre: float32 [2048, 5632], P(('gr', 'fs'), 'tp'), may hold values from -6 to 6
- down_pre: float32 [2048, 5632], P(('gr', 'fs'), 'tp'), may hold values from -16 to 16
- gain_post: float32 [2048], P(('gr', 'fs')), may hold values from 0.1 to 1.9
- gate_post: float32 [2048, 5632], P(('gr', 'fs'), 'tp'), may hold values from -6 to 6
- up_post: float32 [2048, 5632], P(('gr', 'fs'), 'tp'), may hold values from -6 to 6
- down_post: float32 [2048, 5632], P(('gr', 'fs'), 'tp'), may hold values from -16 to 16
Outputs:
- result: bfloat16 [8192, 2048], P(('gr', 'tp'), 'fs')
- gate_first: bfloat16 [5632, 2048], P('fs')
- up_first: bfloat16 [5632, 2048], P('fs')
- down_first: bfloat16 [5632, 2048], P('fs')
- gate_second: bfloat16 [5632, 2048], P('fs')
- up_second: bfloat16 [5632, 2048], P('fs')
- down_second: bfloat16 [5632, 2048], P('fs')
All inputs are finite; a program needn't handle non-finite values.
Results may differ from a plain program's by a relative error of at most 0.028.
Values may be sent and summed in bfloat16 or wider, within the bound.
A program may use at most 64 MiB of HBM per device.

v0:
```python
import jax
import jax.numpy as jnp
from jax import lax
from jax.sharding import PartitionSpec as P

D = 2048
FF = 5632
norm_eps = 1e-06


def half_step(tokens_t, w_gate, w_up, w_down):
    whole = lax.all_gather(tokens_t, "fs", axis=0, tiled=True)
    widened = whole.astype(jnp.float32)
    row_scale = lax.rsqrt(jnp.sum(widened * widened, axis=0, keepdims=True) / D + norm_eps) * D ** (
        -0.5
    )
    g = jnp.dot(w_gate, whole, preferred_element_type=jnp.float32) * row_scale
    u = jnp.dot(w_up, whole, preferred_element_type=jnp.float32) * row_scale
    hidden = (jax.nn.silu(g) * u).astype(jnp.bfloat16)
    partial_value = lax.dot_general(
        w_down, hidden, (((0,), (0,)), ((), ())), preferred_element_type=jnp.float32
    )
    summed = lax.psum_scatter(
        partial_value.astype(jnp.bfloat16), "fs", scatter_dimension=0, tiled=True
    )
    return (tokens_t.astype(jnp.float32) + 0.5 * FF ** (-0.5) * summed.astype(jnp.float32)).astype(
        jnp.bfloat16
    )


def relayout(matrices):
    m = jnp.stack(matrices)
    m = m.reshape(6, 8, 4, 704).transpose(1, 0, 2, 3)
    m = lax.all_to_all(m, "tp", 0, 0, tiled=True)
    m = m.reshape(8, 6, 4, 4, 176).transpose(0, 3, 1, 2, 4).reshape(32, 24, 176)
    m = lax.all_to_all(m, "fs", 0, 0, tiled=True)
    m = lax.all_gather(m.reshape(32 * 24, 176), ("gr", "tp"), axis=0, tiled=True)
    m = m.reshape(2, 8, 32, 6, 4, 176).transpose(3, 5, 0, 2, 1, 4).reshape(6, 176, 2048)
    return tuple((m[i] for i in range(6)))


def local(prompt, gain_pre, gate_pre, up_pre, down_pre, gain_post, gate_post, up_post, down_post):
    rounded = (
        (gain_pre[:, None] * gate_pre).astype(jnp.bfloat16),
        (gain_pre[:, None] * up_pre).astype(jnp.bfloat16),
        down_pre.astype(jnp.bfloat16),
        (gain_post[:, None] * gate_post).astype(jnp.bfloat16),
        (gain_post[:, None] * up_post).astype(jnp.bfloat16),
        down_post.astype(jnp.bfloat16),
    )
    served = relayout(rounded)
    middle = half_step(prompt.T, served[0], served[1], served[2])
    result = half_step(middle, served[3], served[4], served[5])
    return (result.T, *served)


def solution(mesh):
    rows = P(("gr", "fs"))
    block = P(("gr", "fs"), "tp")
    tokens = P(("gr", "tp"), "fs")
    return jax.shard_map(
        local,
        mesh=mesh,
        in_specs=(tokens, rows, block, block, block, rows, block, block, block),
        out_specs=(tokens,) + (P("fs", None),) * 6,
        check_vma=False,
    )
```

profile of v0, /device:TPU:4, one launch (start us, length us, event | category | flops | bytes accessed | tf_op | source)
XLA Modules:
  0.0 1139.2 jit_solution(12735316528702089241)
XLA Ops:
  7.2 0.0 all-gather.6.cloned.1.call-start
  7.2 0.7 all-gather.6.cloned.1.call-update
  7.9 0.0 all-gather.4.cloned.1.call-start
  7.9 1.0 multiply_convert_fusion.2
  9.0 0.9 convert_element_type.57
  10.0 1.0 multiply_convert_fusion
  11.1 0.9 convert_element_type.60
  12.2 13.6 %all_to_all.10 = bf16[8,6,4,704]{3,2,1,0:T(4,128)(2,1)S(1)} all-to-all(bf16[8,6,4,704]{3,2,1,0:T(4,128)(2,1)S(1)} %bitcast.39), channel_id=1, replica_groups=mesh['gr'=2,'fs'=32,'tp'=8] {'tp'}, dimensions={0} | all-to-all | bytes 540672 | tf_op jit(solution)/shard_map/all_to_all | solution.py:34
  25.8 0.1 copy.47
  25.9 0.3 reshape.74
  26.2 0.2 reshape.78
  26.4 0.2 copy.61
  26.6 37.4 %all_to_all.11 = bf16[32,24,176]{2,1,0:T(8,128)(2,1)} all-to-all(bf16[32,24,176]{2,1,0:T(8,128)(2,1)S(1)} %copy.61), channel_id=1, replica_groups=mesh['gr'=2,'fs'=32,'tp'=8] {'fs'}, dimensions={0} | all-to-all | bytes 540672 | tf_op jit(solution)/shard_map/all_to_all | solution.py:36
  64.0 0.0 all-gather.4.cloned.1.call-update
  64.1 0.0 reduce-scatter.3.cloned.1.call-start
  64.1 174.1 %all-gather.6.cloned.1.call-done = bf16[2048,512]{1,0:T(8,128)(2,1)} async-done(((bf16[64,512]{1,0:T(8,128)(2,1)}), bf16[2048,512]{1,0:T(8,128)(2,1)}) %all-gather.6.cloned.1.call-update) | async-done | bytes 2097168 | tf_op jit(solution)/shard_map/all_gather | solution.py:12
  238.2 2.1 multiply_reduce_fusion.1
  240.3 147.0 %all-gather.4.cloned.1.call-done = bf16[12288,176]{1,0:T(8,128)(2,1)} async-done(((bf16[768,176]{1,0:T(8,128)(2,1)}), bf16[12288,176]{1,0:T(8,128)(2,1)}) %all-gather.4.cloned.1.call-update) | async-done | bytes 4325392 | tf_op jit(solution)/shard_map/all_gather | solution.py:37
  387.3 9.9 reshape.77
  397.2 6.0 fusion.21
  403.2 1.6 copy.50
  404.8 2.5 squeeze.19
  407.3 2.8 copy.49
  410.1 2.5 squeeze.18
  412.6 2.8 copy.51
  415.4 2.5 squeeze.20
  417.9 2.5 convolution_multiply_fusion.3
  420.4 4.8 convolution_convert_fusion.1
  425.2 0.0 reduce-scatter.3.cloned.1.call-update
  425.2 0.0 all-gather.8.cloned.1.call-start
  425.3 238.4 %reduce-scatter.3.cloned.1.call-done = bf16[64,512]{1,0:T(8,128)(2,1)} async-done(((bf16[2048,512]{1,0:T(8,128)(2,1)}), bf16[64,512]{1,0:T(8,128)(2,1)}) %reduce-scatter.3.cloned.1.call-update) | async-done | bytes 65552 | tf_op jit(solution)/shard_map/reduce_scatter | solution.py:23
  663.7 0.0 copy-done.11
  663.7 1.5 add_convert_fusion.1
  665.2 0.0 all-gather.8.cloned.1.call-update
  665.2 0.2 reduce-scatter.5.cloned.1.call-start
  665.5 1.6 copy.53
  667.0 1.7 squeeze.22
  668.7 0.0 copy-start.3
  668.7 1.6 copy.52
  670.3 1.7 squeeze.21
  672.0 0.0 copy-start.5
  672.0 1.6 copy.54
  673.6 1.7 squeeze.23
  675.3 0.0 copy-start.7
  675.3 205.9 %all-gather.8.cloned.1.call-done = bf16[2048,512]{1,0:T(8,128)(2,1)} async-done(((bf16[64,512]{1,0:T(8,128)(2,1)}), bf16[2048,512]{1,0:T(8,128)(2,1)}) %all-gather.8.cloned.1.call-update) | async-done | bytes 2097168 | tf_op jit(solution)/shard_map/all_gather | solution.py:12
  881.3 2.2 multiply_reduce_fusion
  883.5 0.0 copy-done.3
  883.5 0.0 copy-done.9
  883.5 0.6 convolution_multiply_fusion.1
  884.1 0.0 copy-done.5
  884.1 0.0 copy-done.7
  884.1 4.2 convolution_convert_fusion
  888.3 0.0 reduce-scatter.5.cloned.1.call-update
  888.3 1.2 copy-done
  889.5 1.2 copy.55
  890.7 1.2 copy.56
  891.9 0.0 copy-done.1
  892.0 1.2 copy.57
  893.2 1.2 copy.58
  894.4 0.0 copy-done.8
  894.4 1.2 copy.59
  895.6 1.2 copy.60
  896.8 234.4 %reduce-scatter.5.cloned.1.call-done = bf16[64,512]{1,0:T(8,128)(2,1)} async-done(((bf16[2048,512]{1,0:T(8,128)(2,1)}), bf16[64,512]{1,0:T(8,128)(2,1)}) %reduce-scatter.5.cloned.1.call-update) | async-done | bytes 65552 | tf_op jit(solution)/shard_map/reduce_scatter | solution.py:23
  1131.1 1.5 fusion.18
  (27 shorter events, 0.3 us)
Async XLA Ops:
  7.2 231.0 %all-gather.6.cloned.1.call-start = ((), (), s32[]{:S(2)}) async-start(), calls=%async_computation.5 | async-start | bytes 2162688 | tf_op jit(solution)/shard_map/all_gather | solution.py:12
  7.9 379.4 %all-gather.4.cloned.1.call-start = ((), (), s32[]{:S(2)}) async-start(), calls=%async_computation.4 | async-start | bytes 6684672 | tf_op jit(solution)/shard_map/all_gather | solution.py:37
  64.1 599.7 %reduce-scatter.3.cloned.1.call-start = ((), (), s32[]{:S(2)}) async-start(), calls=%async_computation.6 | async-start | bytes 2162688 | tf_op jit(solution)/shard_map/reduce_scatter | solution.py:23
  425.2 238.5 %copy-start.11 = (bf16[512,64]{0,1:T(8,128)(2,1)S(1)}, bf16[512,64]{0,1:T(8,128)(2,1)}, u32[]{:S(2)}) copy-start(bf16[512,64]{0,1:T(8,128)(2,1)} %param.9) | copy-start | bytes 196612
  425.2 456.0 %all-gather.8.cloned.1.call-start = ((), (), s32[]{:S(2)}) async-start(), calls=%async_computation.7 | async-start | bytes 2162688 | tf_op jit(solution)/shard_map/all_gather | solution.py:12
  665.2 465.9 %reduce-scatter.5.cloned.1.call-start = ((), (), s32[]{:S(2)}) async-start(), calls=%async_computation.8 | async-start | bytes 2162688 | tf_op jit(solution)/shard_map/reduce_scatter | solution.py:23
  668.7 214.8 %copy-start.3 = (bf16[176,2048]{0,1:T(8,128)(2,1)}, bf16[176,2048]{0,1:T(8,128)(2,1)S(1)}, u32[]{:S(2)}) copy-start(bf16[176,2048]{0,1:T(8,128)(2,1)S(1)} %squeeze.22) | copy-start | bytes 2162692
  672.0 212.1 %copy-start.5 = (bf16[176,2048]{0,1:T(8,128)(2,1)}, bf16[176,2048]{0,1:T(8,128)(2,1)S(1)}, u32[]{:S(2)}) copy-start(bf16[176,2048]{0,1:T(8,128)(2,1)S(1)} %squeeze.21) | copy-start | bytes 2162692
  675.3 208.8 %copy-start.7 = (bf16[176,2048]{0,1:T(8,128)(2,1)}, bf16[176,2048]{0,1:T(8,128)(2,1)S(1)}, u32[]{:S(2)}) copy-start(bf16[176,2048]{0,1:T(8,128)(2,1)S(1)} %squeeze.23) | copy-start | bytes 2162692
  881.3 2.3 copy-start.9
  888.3 1.2 copy-start
  888.3 2.4 copy-start.2
  889.5 2.4 copy-start.1
  890.7 2.4 copy-start.4
  891.9 2.4 copy-start.8
  893.2 2.4 copy-start.6
  894.4 236.8 %copy-start.10 = (bf16[64,512]{1,0:T(8,128)(2,1)S(1)}, bf16[64,512]{1,0:T(8,128)(2,1)}, u32[]{:S(2)}) copy-start(bf16[64,512]{1,0:T(8,128)(2,1)} %add_convert_fusion.1) | copy-start | bytes 196612
Sparse Core Ops, SparseCore 0:
  10.1 228.0 all-gather.5
  241.5 145.7 all-gather.3
  425.4 238.3 reduce-scatter.2
  666.2 214.9 all-gather.7
  888.4 242.6 reduce-scatter.4
where the time goes:
time: 1140 us
  waiting for transfers between devices  1000 us (88%)
  blocking collectives  51 us (4%)
  local copies, waits for them, and re-layouts  50 us (4%)
  between operations  14 us (1%)
  matrix products  12.1 us (1%)
    reduce_scatter x2, waiting for transfers between devices, half_step(): lax.psum_scatter(partial_value.astype(jnp.bfloat16), 'fs', scatter_dimens...  473 us
    all_gather x2, waiting for transfers between devices, half_step(): whole = lax.all_gather(tokens_t, 'fs', axis=0, tiled=True)  380 us
    all_gather x1, waiting for transfers between devices, relayout(): lax.all_gather(m.reshape(32 * 24, 176), ('gr', 'tp'), axis=0, tiled=True)  147 us
    all_to_all x1, blocking collectives, relayout(): m = lax.all_to_all(m, 'fs', 0, 0, tiled=True)  37.4 us
  transfers between devices with their start and end apart: 5, of which 5 were waited for; matrix products, arithmetic and copies ran while one was open for 2% of the time, Pallas kernels for 0%

commit v1 on v0

--- a/solution.py
+++ b/solution.py
@@ -9,7 +9,9 @@
 
 
 def half_step(tokens_t, w_gate, w_up, w_down):
-    whole = lax.all_gather(tokens_t, "fs", axis=0, tiled=True)
+    whole = jnp.concatenate(
+        lax.all_to_all(jnp.stack([tokens_t] * lax.axis_size("fs")), "fs", 0, 0), axis=0
+    )
     widened = whole.astype(jnp.float32)
     row_scale = lax.rsqrt(jnp.sum(widened * widened, axis=0, keepdims=True) / D + norm_eps) * D ** (
         -0.5

time: 1140 us -> 876 us (0.77)
  the two profiles are of different devices: /device:TPU:4 before, /device:TPU:6 now
where the time goes in v1:
time: 876 us; the launch traced here: 875 us
  waiting for transfers between devices  723 us (83%)
  local copies, waits for them, and re-layouts  58.3 us (7%)
  blocking collectives  50.3 us (6%)
  between operations  13.9 us (2%)
  matrix products  12.2 us (1%)
  starting transfers between devices  10.2 us (1%)
    reduce_scatter x2, waiting for transfers between devices, half_step(): lax.psum_scatter(partial_value.astype(jnp.bfloat16), 'fs', scatter_dimens...  495 us
    all_to_all x2, waiting for transfers between devices, half_step(): lax.all_to_all(jnp.stack([tokens_t] * lax.axis_size('fs')), 'fs', 0, 0)  224 us
    all_to_all x1, blocking collectives, relayout(): m = lax.all_to_all(m, 'fs', 0, 0, tiled=True)  36.2 us
    slice x7, local copies, waits for them, and re-layouts, relayout(): return tuple((m[i] for i in range(6)))  20.6 us
  transfers between devices with their start and end apart: 5, of which 5 were waited for; matrix products, arithmetic and copies ran while one was open for 3% of the time, Pallas kernels for 0%

profile of v1, /device:TPU:6, one launch (start us, length us, event | category | flops | bytes accessed | tf_op | source)
XLA Modules:
  0.0 875.1 jit_solution(16320196857466334367)
XLA Ops:
  7.2 1.0 multiply_convert_fusion.2
  8.3 0.9 convert_element_type.59
  9.2 1.0 multiply_convert_fusion
  10.3 0.9 convert_element_type.62
  11.4 0.0 copy-start.7
  11.4 14.1 %all_to_all.20 = bf16[8,6,4,704]{3,2,1,0:T(4,128)(2,1)S(1)} all-to-all(bf16[8,6,4,704]{3,2,1,0:T(4,128)(2,1)S(1)} %bitcast.45), channel_id=1, replica_groups=mesh['gr'=2,'fs'=32,'tp'=8] {'tp'}, dimensions={0} | all-to-all | bytes 540672 | tf_op jit(solution)/shard_map/all_to_all | solution.py:36
  25.5 0.1 copy.61
  25.6 0.3 reshape.84
  25.9 0.2 reshape.90
  26.1 0.2 copy.75
  26.4 36.2 %all_to_all.21 = bf16[32,24,176]{2,1,0:T(8,128)(2,1)} all-to-all(bf16[32,24,176]{2,1,0:T(8,128)(2,1)S(1)} %copy.75), channel_id=1, replica_groups=mesh['gr'=2,'fs'=32,'tp'=8] {'fs'}, dimensions={0} | all-to-all | bytes 540672 | tf_op jit(solution)/shard_map/all_to_all | solution.py:38
  62.6 0.0 copy-done.7
  62.6 1.6 stack.25
  64.1 5.8 all-to-all-start.2
  70.0 0.0 all-gather.2.cloned.1.call-start
  70.0 0.7 all-gather.2.cloned.1.call-update
  70.7 0.0 reduce-scatter.3.cloned.1.call-start
  70.8 167.8 %all-to-all-done.2 = bf16[32,64,512]{2,1,0:T(8,128)(2,1)S(1)} async-done(((bf16[32,64,512]{2,1,0:T(8,128)(2,1)}), bf16[32,64,512]{2,1,0:T(8,128)(2,1)S(1)}, u32[]{:S(2)}, u32[]{:S(2)}) %all-to-all-start.2) | async-done | bytes 2097184 | tf_op jit(solution)/shard_map/all_to_all | solution.py:13
  238.6 0.6 multiply_reduce_fusion.1
  239.1 3.7 all-gather.2.cloned.1.call-done
  242.8 9.9 %reshape.87 = bf16[2,8,32,6,4,176]{5,4,3,2,1,0:T(4,128)(2,1)} reshape(bf16[12288,176]{1,0:T(8,128)(2,1)} %all-gather.2.cloned.1.call-done) | data formatting | bytes 8650752 | tf_op jit(solution)/shard_map/reshape | solution.py:40
  252.7 6.2 fusion.21
  258.9 1.6 copy.64
  260.5 2.5 squeeze.19
  263.0 2.8 copy.63
  265.8 2.5 squeeze.18
  268.2 2.8 copy.65
  271.0 2.5 squeeze.20
  273.5 2.5 convolution_multiply_fusion.3
  276.0 4.2 convolution_convert_fusion.1
  280.2 0.0 reduce-scatter.3.cloned.1.call-update
  280.3 259.3 %reduce-scatter.3.cloned.1.call-done = bf16[64,512]{1,0:T(8,128)(2,1)} async-done(((bf16[2048,512]{1,0:T(8,128)(2,1)}), bf16[64,512]{1,0:T(8,128)(2,1)}) %reduce-scatter.3.cloned.1.call-update) | async-done | bytes 65552 | tf_op jit(solution)/shard_map/reduce_scatter | solution.py:25
  539.6 0.9 add_convert_fusion.1
  540.5 1.6 stack.26
  542.0 4.0 all-to-all-start.3
  546.1 0.2 reduce-scatter.5.cloned.1.call-start
  546.3 2.9 copy.67
  549.1 2.5 squeeze.22
  551.6 2.8 copy.66
  554.5 2.5 squeeze.21
  556.9 1.6 copy.68
  558.6 0.0 copy-start.3
  558.6 2.6 squeeze.23
  561.2 55.8 %all-to-all-done.3 = bf16[32,64,512]{2,1,0:T(8,128)(2,1)S(1)} async-done(((bf16[32,64,512]{2,1,0:T(8,128)(2,1)}), bf16[32,64,512]{2,1,0:T(8,128)(2,1)S(1)}, u32[]{:S(2)}, u32[]{:S(2)}) %all-to-all-start.3) | async-done | bytes 2097184 | tf_op jit(solution)/shard_map/all_to_all | solution.py:13
  617.0 0.6 multiply_reduce_fusion
  617.6 0.0 copy-done.3
  617.6 1.3 convolution_multiply_fusion.1
  618.9 4.2 convolution_convert_fusion
  623.1 0.0 copy-start
  623.1 0.0 reduce-scatter.5.cloned.1.call-update
  623.1 1.2 copy-done
  624.3 1.2 copy.69
  625.5 0.0 copy-done.2
  625.5 1.2 copy.70
  626.7 0.0 copy-done.1
  626.7 1.2 copy.71
  627.9 0.0 copy-done.4
  627.9 1.2 copy.72
  629.1 0.0 copy-done.6
  629.2 1.2 copy.73
  630.4 0.0 copy-done.5
  630.4 1.2 copy.74
  631.6 235.5 %reduce-scatter.5.cloned.1.call-done = bf16[64,512]{1,0:T(8,128)(2,1)} async-done(((bf16[2048,512]{1,0:T(8,128)(2,1)}), bf16[64,512]{1,0:T(8,128)(2,1)}) %reduce-scatter.5.cloned.1.call-update) | async-done | bytes 65552 | tf_op jit(solution)/shard_map/reduce_scatter | solution.py:25
  867.0 1.5 fusion.18
  (19 shorter events, 0.3 us)
Async XLA Ops:
  11.4 51.2 %copy-start.7 = (bf16[512,64]{0,1:T(8,128)(2,1)S(1)}, bf16[512,64]{0,1:T(8,128)(2,1)}, u32[]{:S(2)}) copy-start(bf16[512,64]{0,1:T(8,128)(2,1)} %param.9) | copy-start | bytes 196612
  64.1 174.4 %all-to-all-start.2 = ((bf16[32,64,512]{2,1,0:T(8,128)(2,1)}), bf16[32,64,512]{2,1,0:T(8,128)(2,1)S(1)}, u32[]{:S(2)}, u32[]{:S(2)}) async-start(bf16[32,64,512]{2,1,0:T(8,128)(2,1)} %stack.25), calls=%async_computation.2 | async-start | bytes 4194304 | tf_op jit(solution)/shard_map/all_to_all | solution.py:13
  70.0 172.8 %all-gather.2.cloned.1.call-start = ((), (), s32[]{:S(2)}) async-start(), calls=%async_computation.6 | async-start | bytes 6684672 | tf_op jit(solution)/shard_map/all_gather | solution.py:39
  70.7 468.9 %reduce-scatter.3.cloned.1.call-start = ((), (), s32[]{:S(2)}) async-start(), calls=%async_computation.7 | async-start | bytes 2162688 | tf_op jit(solution)/shard_map/reduce_scatter | solution.py:25
  542.0 75.0 %all-to-all-start.3 = ((bf16[32,64,512]{2,1,0:T(8,128)(2,1)}), bf16[32,64,512]{2,1,0:T(8,128)(2,1)S(1)}, u32[]{:S(2)}, u32[]{:S(2)}) async-start(bf16[32,64,512]{2,1,0:T(8,128)(2,1)} %stack.26), calls=%async_computation.4 | async-start | bytes 4194304 | tf_op jit(solution)/shard_map/all_to_all | solution.py:13
  546.1 321.0 %reduce-scatter.5.cloned.1.call-start = ((), (), s32[]{:S(2)}) async-start(), calls=%async_computation.8 | async-start | bytes 2162688 | tf_op jit(solution)/shard_map/reduce_scatter | solution.py:25
  558.6 59.0 %copy-start.3 = (bf16[176,2048]{0,1:T(8,128)(2,1)S(1)}, bf16[176,2048]{0,1:T(8,128)(2,1)}, u32[]{:S(2)}) copy-start(bf16[176,2048]{0,1:T(8,128)(2,1)} %squeeze.22) | copy-start | bytes 2162692
  623.1 1.2 copy-start
  623.1 2.4 copy-start.2
  624.3 2.4 copy-start.1
  625.5 2.4 copy-start.4
  626.7 2.4 copy-start.6
  627.9 2.4 copy-start.5
Sparse Core Ops, SparseCore 0:
  74.1 168.6 all-gather.1
  280.4 259.1 reduce-scatter.2
  623.2 243.7 reduce-scatter.4
